TPU v7x, 32 devices: a whole 2x2x4 slice. The times are simulated.
32 devices in a mesh: sp: 8 (over z, x), tp: 4 (over y, core).
Axes of the slice: x: 2, y: 2, z: 4, core: 2. Of those that a mesh axis runs over, the one named last changes fastest.
Arguments:
- skip_stream_input: bfloat16 [1024, 2048], P('sp'), may hold values from -16 to 16
- asking_vectors_split: bfloat16 [1024, 2048], P('sp', 'tp'), may hold values from -8 to 8
- lookup_vectors_split: bfloat16 [1024, 512], P('sp'), may hold values from -8 to 8
- content_vectors_split: bfloat16 [1024, 512], P('sp'), may hold values from -6 to 6
- asking_rms_gain: float32 [128], replicated, may hold values from 0.1 to 1.9
- lookup_rms_gain: float32 [128], replicated, may hold values from 0.1 to 1.9
- softness_per_channel: float32 [16], P('tp'), may hold values from 1.5 to 24
- mixing_exit_weights: bfloat16 [2048, 2048], P('tp'), may hold values from -0.125 to 0.125
- specialist_rms_gain: float32 [2048], replicated, may hold values from 0.1 to 1.9
- selected_dispatch_weights: float32 [1024, 2], P('sp'), may hold values from -6 to 6
- selected_specialist_ids: int32 [1024, 2], P('sp'), may hold values from 0 to 7, all different within a row; in each aligned block of 128 rows (0 to 127, 128 to 255, ...) at most 48 rows name the same one
- specialist_switch_weights: bfloat16 [8, 2048, 2048], P('sp', None, 'tp'), may hold values from -0.125 to 0.125
- specialist_widen_weights: bfloat16 [8, 2048, 2048], P('sp', None, 'tp'), may hold values from -0.125 to 0.125
- specialist_shrink_weights: bfloat16 [8, 2048, 2048], P('sp', 'tp'), may hold values from -0.125 to 0.125
Outputs:
- layer_out: bfloat16 [1024, 2048], P('sp', 'tp')
Inputs may be any that keep to these rules, and one draw needn't show every extreme that they name: `selected_specialist_ids`: each row names 2 different experts. In each aligned block of 128 rows no expert is named by more than 48 rows, a bound that some block reaches.
All inputs are finite; a program needn't handle non-finite values.
Results may differ from a plain program's by a relative error of at most 0.0085.
Values may be sent and summed in bfloat16 or wider, within the bound.
A program may use at most 64 MiB of HBM per device.

v0:
```python
import math
import jax
import jax.numpy as jnp
from jax import lax
from jax.sharding import PartitionSpec as P

CHANNEL_WIDTH = 128
GROUP = 4
GRID_W = 64
EPSILON = 1e-06
NEGATIVE = -1e30


def rotate_half(values_in, positions, full_width):
    half_width = full_width // 2
    frequency = 10000.0 ** (-jnp.arange(half_width, dtype=jnp.float32) / half_width)
    angles = positions.astype(jnp.float32)[:, None] * frequency[None, :]
    cosine = jnp.cos(angles)[:, None, :]
    sine = jnp.sin(angles)[:, None, :]
    leading = values_in[..., :half_width]
    trailing = values_in[..., half_width:]
    return jnp.concatenate(
        [leading * cosine - trailing * sine, trailing * cosine + leading * sine], axis=-1
    )


def norm_rotate(heads_in, gain_vec, positions):
    widened = heads_in.astype(jnp.float32)
    scaled = (
        widened
        * lax.rsqrt(jnp.mean(widened * widened, axis=-1, keepdims=True) + EPSILON)
        * gain_vec
    )
    half_width = scaled.shape[-1] // 2
    grid_rows = positions // GRID_W
    grid_cols = positions % GRID_W
    turned = jnp.concatenate(
        [
            rotate_half(scaled[..., :half_width], grid_rows, half_width),
            rotate_half(scaled[..., half_width:], grid_cols, half_width),
        ],
        axis=-1,
    )
    return turned.astype(jnp.bfloat16)


def shards(
    skip_stream_input,
    asking_vectors_split,
    lookup_vectors_split,
    content_vectors_split,
    asking_rms_gain,
    lookup_rms_gain,
    softness_per_channel,
    mixing_exit_weights,
    specialist_rms_gain,
    selected_dispatch_weights,
    selected_specialist_ids,
    specialist_switch_weights,
    specialist_widen_weights,
    specialist_shrink_weights,
):
    tok_count = skip_stream_input.shape[0]
    model_width = skip_stream_input.shape[1]
    heads_here = asking_vectors_split.shape[1] // CHANNEL_WIDTH
    local_key_value_heads = max(1, heads_here // GROUP)
    local_group_count = heads_here // local_key_value_heads
    tp_position = lax.axis_index("tp")
    positions = lax.axis_index("sp") * tok_count + jnp.arange(tok_count, dtype=jnp.int32)
    query_turned = norm_rotate(
        asking_vectors_split.reshape(tok_count, heads_here, CHANNEL_WIDTH),
        asking_rms_gain,
        positions,
    )
    first_head = tp_position * heads_here // GROUP
    key_cols = lax.dynamic_slice_in_dim(
        lookup_vectors_split, first_head * CHANNEL_WIDTH, local_key_value_heads * CHANNEL_WIDTH, 1
    )
    value_cols = lax.dynamic_slice_in_dim(
        content_vectors_split, first_head * CHANNEL_WIDTH, local_key_value_heads * CHANNEL_WIDTH, 1
    )
    key_turned = norm_rotate(
        key_cols.reshape(tok_count, local_key_value_heads, CHANNEL_WIDTH),
        lookup_rms_gain,
        positions,
    )
    key_turned = key_turned.reshape(tok_count, local_key_value_heads * CHANNEL_WIDTH)
    query_grouped = query_turned.reshape(
        tok_count, local_key_value_heads, local_group_count, CHANNEL_WIDTH
    ).transpose(1, 2, 0, 3)
    inverse_root_width = (softness_per_channel / math.sqrt(CHANNEL_WIDTH)).reshape(
        local_key_value_heads, local_group_count, 1, 1
    )

    def absorb(run_state, key_span, value_span):
        run_max, run_sum, run_acc = run_state
        scores = (
            jnp.einsum(
                "kgqd,nkd->kgqn", query_grouped, key_span, preferred_element_type=jnp.float32
            )
            * inverse_root_width
        )
        new_max = jnp.maximum(run_max, jnp.max(scores, axis=-1))
        factor = jnp.exp(run_max - new_max)
        exp_terms = jnp.exp(scores - new_max[..., None])
        run_sum = run_sum * factor + jnp.sum(exp_terms, axis=-1)
        run_acc = run_acc * factor[..., None] + jnp.einsum(
            "kgqn,nkd->kgqd",
            exp_terms.astype(jnp.bfloat16),
            value_span,
            preferred_element_type=jnp.float32,
        )
        return (new_max, run_sum, run_acc)

    initial = (
        jnp.full((local_key_value_heads, local_group_count, tok_count), NEGATIVE, jnp.float32),
        jnp.zeros((local_key_value_heads, local_group_count, tok_count), jnp.float32),
        jnp.zeros(
            (local_key_value_heads, local_group_count, tok_count, CHANNEL_WIDTH), jnp.float32
        ),
    )
    key_piece = lax.all_gather(key_turned, "sp", axis=0, tiled=True)
    value_piece = lax.all_gather(value_cols, "sp", axis=0, tiled=True)
    piece_len = key_piece.shape[0]
    span_len = 1024
    span_count = piece_len // span_len
    key_spans = key_piece.reshape(span_count, span_len, local_key_value_heads, CHANNEL_WIDTH)
    value_spans = value_piece.reshape(span_count, span_len, local_key_value_heads, CHANNEL_WIDTH)

    def step_span(inner_state, span_pair):
        return (absorb(inner_state, span_pair[0], span_pair[1]), None)

    result_state, unused = lax.scan(step_span, initial, (key_spans, value_spans))
    final_max, final_sum, final_acc = result_state
    attn_heads = (final_acc / final_sum[..., None]).astype(jnp.bfloat16)
    attn_flat = attn_heads.transpose(2, 0, 1, 3).reshape(tok_count, heads_here * CHANNEL_WIDTH)
    partial_sum = jnp.dot(attn_flat, mixing_exit_weights, preferred_element_type=jnp.float32)
    share_width = model_width // lax.axis_size("tp")
    first_col = tp_position * share_width
    attended = lax.psum(partial_sum.astype(jnp.bfloat16), "tp")
    mid_rows = (skip_stream_input.astype(jnp.float32) + attended.astype(jnp.float32)).astype(
        jnp.bfloat16
    )
    mid_wide = mid_rows.astype(jnp.float32)
    normed_rows = (
        mid_wide
        * lax.rsqrt(jnp.mean(mid_wide * mid_wide, axis=-1, keepdims=True) + EPSILON)
        * specialist_rms_gain
    ).astype(jnp.bfloat16)
    mid_share = lax.dynamic_slice_in_dim(mid_rows, first_col, share_width, 1)
    outgoing_rows = lax.dynamic_slice_in_dim(normed_rows, first_col, share_width, 1)
    experts_count = lax.axis_size("sp")
    top_count = selected_specialist_ids.shape[1]
    capacity = max(2, 3 * tok_count * top_count // (2 * experts_count))
    flat_ids = selected_specialist_ids.reshape(-1)
    one_hot = (flat_ids[:, None] == jnp.arange(experts_count, dtype=jnp.int32)[None, :]).astype(
        jnp.int32
    )
    earlier = jnp.cumsum(one_hot, axis=0) - one_hot
    slot_index = jnp.sum(earlier * one_hot, axis=1)
    destination = flat_ids * capacity + slot_index
    owner_rows = jnp.arange(tok_count * top_count, dtype=jnp.int32) // top_count
    slot_owner = jnp.zeros((experts_count * capacity,), jnp.int32).at[destination].set(owner_rows)
    filled = jnp.zeros((experts_count * capacity,), jnp.int32).at[destination].set(1)
    outgoing = jnp.where(
        filled[:, None] > 0, outgoing_rows[slot_owner], jnp.zeros((), jnp.bfloat16)
    )
    outgoing = outgoing.reshape(experts_count, capacity, outgoing_rows.shape[1])
    gate_local = specialist_switch_weights[0]
    up_local = specialist_widen_weights[0]
    down_local = specialist_shrink_weights[0]
    arrived = lax.all_to_all(outgoing, "sp", split_axis=0, concat_axis=0, tiled=True)
    row_count = arrived.shape[0] * arrived.shape[1]
    feature_piece = lax.all_gather(arrived, "tp", axis=2, tiled=True)
    piece_width = feature_piece.shape[2]
    flat_piece = feature_piece.reshape(row_count, piece_width)
    gate_acc = jnp.dot(flat_piece, gate_local, preferred_element_type=jnp.float32)
    up_acc = jnp.dot(flat_piece, up_local, preferred_element_type=jnp.float32)
    hidden = (jax.nn.silu(gate_acc) * up_acc).astype(jnp.bfloat16)
    expert_part = jnp.dot(hidden, down_local, preferred_element_type=jnp.float32)
    expert_part = expert_part.reshape(arrived.shape[0], arrived.shape[1], model_width)
    expert_share = lax.psum_scatter(
        expert_part.astype(jnp.bfloat16), "tp", scatter_dimension=2, tiled=True
    )
    returned = lax.all_to_all(expert_share, "sp", split_axis=0, concat_axis=0, tiled=True)
    back_flat = returned.reshape(experts_count * capacity, share_width)
    picked = back_flat[destination].reshape(tok_count, top_count, share_width).astype(jnp.float32)
    route_weights = jax.nn.softmax(selected_dispatch_weights, axis=-1)
    layer_out = mid_share.astype(jnp.float32) + jnp.sum(route_weights[..., None] * picked, axis=1)
    return layer_out.astype(jnp.bfloat16)


def solution(mesh):
    in_specs = (
        P("sp", None),
        P("sp", "tp"),
        P("sp", None),
        P("sp", None),
        P(),
        P(),
        P("tp"),
        P("tp", None),
        P(),
        P("sp", None),
        P("sp", None),
        P("sp", None, "tp"),
        P("sp", None, "tp"),
        P("sp", "tp", None),
    )
    out_specs = P("sp", "tp")
    return jax.shard_map(shards, mesh=mesh, in_specs=in_specs, out_specs=out_specs, check_vma=False)
```

profile of v0, /device:TPU:0, one launch (start us, length us, event | category | flops | bytes accessed | tf_op | source)
XLA Modules:
  0.0 204.7 jit_solution(4723165117829957611)
XLA Ops:
  6.6 0.9 constant_dynamic-slice_fusion.1
  9.2 28.3 %all_gather.9 = bf16[1024,128]{0,1:T(8,128)(2,1)S(1)} all-gather(bf16[128,128]{0,1:T(8,128)(2,1)S(1)} %pad_maximum_fusion), channel_id=1, replica_groups=mesh['sp'=8,'tp'=4] {'sp'}, dimensions={0}, use_global_device_ids=true | all-gather | bytes 294912 | tf_op jit(solution)/shard_map/all_gather | solution.py:122
  37.5 1.0 copy.24
  39.4 0.8 multiply_multiply_fusion
  41.1 1.3 copy-done.1
  42.9 0.8 constant_dynamic-slice_fusion
  43.8 26.8 %all_gather.10 = bf16[1024,128]{0,1:T(8,128)(2,1)S(1)} all-gather(bf16[128,128]{0,1:T(8,128)(2,1)S(1)} %copy.36), channel_id=1, replica_groups=mesh['sp'=8,'tp'=4] {'sp'}, dimensions={0}, use_global_device_ids=true | all-gather | bytes 294912 | tf_op jit(solution)/shard_map/all_gather | solution.py:123
  70.7 2.2 %fusion.14 = bf16[4,128,128]{1,2,0:T(8,128)(2,1)S(1)} fusion(f32[4,128,1024]{2,1,0:T(8,128)} %copy-done.1, f32[4,128]{1,0:T(4,128)S(1)} %broadcast_maximum_fusion, f32[4]{0:T(128)S(1)} %broadcast_multiply_fusion.1, bf16[1024,128]{0,1:T(8,128)(2,1)S(1)} %all_gather.10, f32[4,128]{1,0:T(4,128)S(1)} %get-tuple-element.44, f32[4,128]{1,0:T(4,128)S(1)} %get-tuple-element.43), kind=kOutput, calls=%fused_computation.19 | convolution fusion | flops 135987200 | bytes 2496528 | tf_op jit(solution)/shard_map/while/body/eval_jaxpr/kgqn,nkd->kgqd/dot_general | solution.py:107
  72.9 1.3 convolution_convert_fusion.1
  75.9 1.4 scatter_custom_fusion.1
  77.3 1.4 scatter_custom_fusion
  78.8 0.8 dynamic-slice
  79.6 25.8 %all-reduce.2.cloned.1.call-done = bf16[128,2048]{1,0:T(8,128)(2,1)} async-done(((bf16[128,2048]{1,0:T(8,128)(2,1)}), bf16[128,2048]{1,0:T(8,128)(2,1)}) %all-reduce.2.cloned.1.call-update) | async-done | bytes 524304 | tf_op jit(solution)/shard_map/psum | solution.py:140
  105.4 1.3 multiply_reduce_fusion.1
  106.9 2.1 %gather_fusion = bf16[384,512]{1,0:T(8,128)(2,1)S(1)} fusion(bf16[128,512]{1,0:T(8,128)(2,1)S(1)} %fusion.19, s32[1024]{0:T(1024)S(1)} %pad_clamp_fusion.1), kind=kCustom, calls=%fused_computation | custom fusion | bytes 787968 | tf_op jit(solution)/shard_map/gather | solution.py:166
  109.1 16.5 %all_to_all.10 = bf16[8,48,512]{2,1,0:T(8,128)(2,1)} all-to-all(bf16[8,48,512]{2,1,0:T(8,128)(2,1)S(1)} %broadcast_select_fusion), channel_id=1, replica_groups=mesh['sp'=8,'tp'=4] {'sp'}, dimensions={0} | all-to-all | bytes 786432 | tf_op jit(solution)/shard_map/all_to_all | solution.py:172
  125.7 18.0 %all-gather.2.cloned.1.call-done = bf16[8,48,2048]{2,1,0:T(8,128)(2,1)} async-done(((bf16[8,48,512]{2,1,0:T(8,128)(2,1)}), bf16[8,48,2048]{2,1,0:T(8,128)(2,1)}) %all-gather.2.cloned.1.call-update) | async-done | bytes 1572880 | tf_op jit(solution)/shard_map/all_gather | solution.py:174
  143.7 3.2 %fusion.3 = f32[384,512]{1,0:T(8,128)S(1)} fusion(bf16[384,2048]{1,0:T(8,128)(2,1)} %bitcast.82, bf16[1,2048,512]{2,1,0:T(8,128)(2,1)} %param.25), kind=kOutput, calls=%fused_computation.9 | convolution fusion | flops 805306368 | bytes 4456448 | tf_op jit(solution)/shard_map/dot_general | solution.py:177
  146.9 1.0 fusion.10
  147.9 2.1 %convolution_convert_fusion = bf16[8,48,2048]{2,1,0:T(8,128)(2,1)} fusion(bf16[8,48,512]{2,1,0:T(8,128)(2,1)S(1)} %bitcast.84, bf16[1,512,2048]{2,1,0:T(8,128)(2,1)S(1)} %copy-done), kind=kOutput, calls=%fused_computation.4 | convolution fusion | flops 806092800 | bytes 4063232 | tf_op jit(solution)/shard_map/dot_general | solution.py:180
  150.1 28.1 %reduce-scatter.2.cloned.1.call-done = bf16[8,48,512]{2,1,0:T(8,128)(2,1)} async-done(((bf16[8,48,2048]{2,1,0:T(8,128)(2,1)}), bf16[8,48,512]{2,1,0:T(8,128)(2,1)}) %reduce-scatter.2.cloned.1.call-update) | async-done | bytes 393232 | tf_op jit(solution)/shard_map/reduce_scatter | solution.py:182
  178.2 5.5 %all-to-all-start.1 = ((bf16[8,48,512]{2,1,0:T(8,128)(2,1)}), bf16[8,48,512]{2,1,0:T(8,128)(2,1)S(1)}, u32[]{:S(2)}, u32[]{:S(2)}) async-start(bf16[8,48,512]{2,1,0:T(8,128)(2,1)} %reduce-scatter.2.cloned.1.call-done), calls=%async_computation.2 | async-start | bytes 786432 | tf_op jit(solution)/shard_map/all_to_all | solution.py:185
  183.9 11.4 %all-to-all-done.1 = bf16[8,48,512]{2,1,0:T(8,128)(2,1)S(1)} async-done(((bf16[8,48,512]{2,1,0:T(8,128)(2,1)}), bf16[8,48,512]{2,1,0:T(8,128)(2,1)S(1)}, u32[]{:S(2)}, u32[]{:S(2)}) %all-to-all-start.1) | async-done | bytes 393248 | tf_op jit(solution)/shard_map/all_to_all | solution.py:185
  195.3 1.2 gather_fusion.1
  (71 shorter events, 8.1 us)
Async XLA Ops:
  6.5 141.4 %copy-start = (bf16[1,512,2048]{2,1,0:T(8,128)(2,1)S(1)}, bf16[1,512,2048]{2,1,0:T(8,128)(2,1)}, u32[]{:S(2)}) copy-start(bf16[1,512,2048]{2,1,0:T(8,128)(2,1)} %param.27) | copy-start | bytes 6291460
  6.5 98.8 %all-reduce.2.cloned.1.call-start = ((), (), s32[]{:S(2)}) async-start(), calls=%async_computation.3 | async-start | bytes 1048576 | tf_op jit(solution)/shard_map/psum | solution.py:140
  41.1 1.4 copy-start.1
  43.8 29.1 %copy-start.2 = (bf16[512,2048]{1,0:T(8,128)(2,1)S(1)}, bf16[512,2048]{1,0:T(8,128)(2,1)}, u32[]{:S(2)}) copy-start(bf16[512,2048]{1,0:T(8,128)(2,1)} %param.21) | copy-start | bytes 6291460
  72.9 1.4 copy-start.5
  72.9 32.5 %copy-start.3 = (bf16[128,2048]{1,0:T(8,128)(2,1)S(1)}, bf16[128,2048]{1,0:T(8,128)(2,1)}, u32[]{:S(2)}) copy-start(bf16[128,2048]{1,0:T(8,128)(2,1)} %param.14) | copy-start | bytes 1572868
  74.2 69.4 %all-gather.2.cloned.1.call-start = ((), (), s32[]{:S(2)}) async-start(), calls=%async_computation.4 | async-start | bytes 1966080 | tf_op jit(solution)/shard_map/all_gather | solution.py:174
  125.6 52.6 %reduce-scatter.2.cloned.1.call-start = ((), (), s32[]{:S(2)}) async-start(), calls=%async_computation.5 | async-start | bytes 1966080 | tf_op jit(solution)/shard_map/reduce_scatter | solution.py:182
  143.7 3.2 %copy-start.6 = (bf16[1,2048,512]{2,1,0:T(8,128)(2,1)S(1)}, bf16[1,2048,512]{2,1,0:T(8,128)(2,1)}, u32[]{:S(2)}) copy-start(bf16[1,2048,512]{2,1,0:T(8,128)(2,1)} %param.26) | copy-start | bytes 6291460
  143.7 3.2 %copy-start.7 = (bf16[8,48,2048]{2,1,0:T(8,128)(2,1)S(1)}, bf16[8,48,2048]{2,1,0:T(8,128)(2,1)}, u32[]{:S(2)}) copy-start(bf16[8,48,2048]{2,1,0:T(8,128)(2,1)} %all-gather.2.cloned.1.call-done) | copy-start | bytes 4718596
  150.0 33.7 %copy-start.4 = (f32[128,2]{0,1:T(2,128)S(1)}, f32[128,2]{0,1:T(2,128)}, u32[]{:S(2)}) copy-start(f32[128,2]{0,1:T(2,128)} %param.23) | copy-start | bytes 3076
  178.2 17.1 %all-to-all-start.1 = ((bf16[8,48,512]{2,1,0:T(8,128)(2,1)}), bf16[8,48,512]{2,1,0:T(8,128)(2,1)S(1)}, u32[]{:S(2)}, u32[]{:S(2)}) async-start(bf16[8,48,512]{2,1,0:T(8,128)(2,1)} %reduce-scatter.2.cloned.1.call-done), calls=%async_computation.2 | async-start | bytes 786432 | tf_op jit(solution)/shard_map/all_to_all | solution.py:185
Sparse Core Ops, SparseCore 0:
  74.3 30.9 all-reduce.1
  125.8 17.8 all-gather.1
  150.2 27.9 reduce-scatter.1
where the time goes:
time: 205 us
  waiting for transfers between devices  83.3 us (41%)
  blocking collectives  71.7 us (35%)
  between operations  13.5 us (7%)
  local copies, waits for them, and re-layouts  12.6 us (6%)
  matrix products  10.4 us (5%)
  other arithmetic  7.66 us (4%)
  starting transfers between devices  5.57 us (3%)
    all_gather x1, blocking collectives, shards(): key_piece = lax.all_gather(key_turned, 'sp', axis=0, tiled=True)  28.3 us
    reduce_scatter x1, waiting for transfers between devices, shards(): lax.psum_scatter(expert_part.astype(jnp.bfloat16), 'tp', scatter_dimensio...  28.1 us
    all_gather x1, blocking collectives, shards(): value_piece = lax.all_gather(value_cols, 'sp', axis=0, tiled=True)  26.8 us
    psum x1, waiting for transfers between devices, shards(): attended = lax.psum(partial_sum.astype(jnp.bfloat16), 'tp')  25.8 us
    all_gather x1, waiting for transfers between devices, shards(): feature_piece = lax.all_gather(arrived, 'tp', axis=2, tiled=True)  18 us
    all_to_all x1, blocking collectives, shards(): lax.all_to_all(outgoing, 'sp', split_axis=0, concat_axis=0, tiled=True)  16.5 us
    all_to_all x1, waiting for transfers between devices, shards(): lax.all_to_all(expert_share, 'sp', split_axis=0, concat_axis=0, tiled=True)  11.4 us
    all_to_all x1, starting transfers between devices, shards(): lax.all_to_all(expert_share, 'sp', split_axis=0, concat_axis=0, tiled=True)  5.48 us
  transfers between devices with their start and end apart: 4, of which 4 were waited for; matrix products, arithmetic and copies ran while one was open for 3% of the time, Pallas kernels for 0%

commit v1 on v0

--- a/solution.py
+++ b/solution.py
@@ -171,7 +171,7 @@
     down_local = specialist_shrink_weights[0]
     arrived = lax.all_to_all(outgoing, "sp", split_axis=0, concat_axis=0, tiled=True)
     row_count = arrived.shape[0] * arrived.shape[1]
-    feature_piece = lax.all_gather(arrived, "tp", axis=2, tiled=True)
+    feature_piece = jnp.concatenate(lax.all_gather(arrived, "tp"), axis=2)
     piece_width = feature_piece.shape[2]
     flat_piece = feature_piece.reshape(row_count, piece_width)
     gate_acc = jnp.dot(flat_piece, gate_local, preferred_element_type=jnp.float32)

time: 205 us -> 208 us (1.015)
  local copies, waits for them, and re-layouts: 12.6 us -> 17.4 us
  matrix products: 10.4 us -> 8.21 us
    reshape x0 -> x1, local copies, waits for them, and re-layouts: none -> 2.63 us  [shards(): feature_piece = jnp.concatenate(lax.all_gather(arrived, 'tp'), axis=2)]
    dot_general x1, matrix products: 3.18 us -> 0.99 us  [shards(): jnp.dot(flat_piece, gate_local, preferred_element_type=jnp.float32)]
    unnamed x20 -> x21, local copies, waits for them, and re-layouts: 2.73 us -> 4.9 us
where the time goes in v1:
time: 208 us; the launch traced here: 207 us
  waiting for transfers between devices  83.3 us (40%)
  blocking collectives  71.7 us (34%)
  local copies, waits for them, and re-layouts  17.4 us (8%)
  between operations  13.5 us (6%)
  matrix products  8.21 us (4%)
  other arithmetic  7.66 us (4%)
  starting transfers between devices  5.57 us (3%)
    all_gather x1, blocking collectives, shards(): key_piece = lax.all_gather(key_turned, 'sp', axis=0, tiled=True)  28.3 us
    reduce_scatter x1, waiting for transfers between devices, shards(): lax.psum_scatter(expert_part.astype(jnp.bfloat16), 'tp', scatter_dimensio...  28.1 us
    all_gather x1, blocking collectives, shards(): value_piece = lax.all_gather(value_cols, 'sp', axis=0, tiled=True)  26.8 us
    psum x1, waiting for transfers between devices, shards(): attended = lax.psum(partial_sum.astype(jnp.bfloat16), 'tp')  25.8 us
    all_gather x1, waiting for transfers between devices, shards(): feature_piece = jnp.concatenate(lax.all_gather(arrived, 'tp'), axis=2)  18 us
    all_to_all x1, blocking collectives, shards(): lax.all_to_all(outgoing, 'sp', split_axis=0, concat_axis=0, tiled=True)  16.5 us
    all_to_all x1, waiting for transfers between devices, shards(): lax.all_to_all(expert_share, 'sp', split_axis=0, concat_axis=0, tiled=True)  11.4 us
    all_to_all x1, starting transfers between devices, shards(): lax.all_to_all(expert_share, 'sp', split_axis=0, concat_axis=0, tiled=True)  5.48 us
  transfers between devices with their start and end apart: 4, of which 4 were waited for; matrix products, arithmetic and copies ran while one was open for 3% of the time, Pallas kernels for 0%

profile of v1, /device:TPU:0, one launch (start us, length us, event | category | flops | bytes accessed | tf_op | source)
XLA Modules:
  0.0 207.3 jit_solution(14964391127555685979)
XLA Ops:
  6.6 0.9 constant_dynamic-slice_fusion.1
  9.2 28.3 %all_gather.12 = bf16[1024,128]{0,1:T(8,128)(2,1)S(1)} all-gather(bf16[128,128]{0,1:T(8,128)(2,1)S(1)} %pad_maximum_fusion), channel_id=1, replica_groups=mesh['sp'=8,'tp'=4] {'sp'}, dimensions={0}, use_global_device_ids=true | all-gather | bytes 294912 | tf_op jit(solution)/shard_map/all_gather | solution.py:122
  37.5 1.0 copy.40
  39.4 0.8 multiply_multiply_fusion
  41.1 1.3 copy-done.1
  43.8 26.8 %all_gather.13 = bf16[1024,128]{0,1:T(8,128)(2,1)S(1)} all-gather(bf16[128,128]{0,1:T(8,128)(2,1)S(1)} %copy.53), channel_id=1, replica_groups=mesh['sp'=8,'tp'=4] {'sp'}, dimensions={0}, use_global_device_ids=true | all-gather | bytes 294912 | tf_op jit(solution)/shard_map/all_gather | solution.py:123
  70.7 2.2 %fusion.14 = bf16[4,128,128]{1,2,0:T(8,128)(2,1)S(1)} fusion(f32[4,128,1024]{2,1,0:T(8,128)} %copy-done.1, f32[4,128]{1,0:T(4,128)S(1)} %broadcast_maximum_fusion, f32[4]{0:T(128)S(1)} %broadcast_multiply_fusion.1, bf16[1024,128]{0,1:T(8,128)(2,1)S(1)} %all_gather.13, f32[4,128]{1,0:T(4,128)S(1)} %get-tuple-element.44, f32[4,128]{1,0:T(4,128)S(1)} %get-tuple-element.43), kind=kOutput, calls=%fused_computation.19 | convolution fusion | flops 135987200 | bytes 2496528 | tf_op jit(solution)/shard_map/while/body/eval_jaxpr/kgqn,nkd->kgqd/dot_general | solution.py:107
  72.9 1.3 convolution_convert_fusion.1
  75.9 1.4 scatter_custom_fusion.1
  77.3 1.4 scatter_custom_fusion
  79.6 25.8 %all-reduce.2.cloned.1.call-done = bf16[128,2048]{1,0:T(8,128)(2,1)} async-done(((bf16[128,2048]{1,0:T(8,128)(2,1)}), bf16[128,2048]{1,0:T(8,128)(2,1)}) %all-reduce.2.cloned.1.call-update) | async-done | bytes 524304 | tf_op jit(solution)/shard_map/psum | solution.py:140
  105.4 1.3 multiply_reduce_fusion.1
  106.9 2.1 gather_fusion
  109.1 16.5 %all_to_all.10 = bf16[8,48,512]{2,1,0:T(8,128)(2,1)} all-to-all(bf16[8,48,512]{2,1,0:T(8,128)(2,1)S(1)} %broadcast_select_fusion), channel_id=1, replica_groups=mesh['sp'=8,'tp'=4] {'sp'}, dimensions={0} | all-to-all | bytes 786432 | tf_op jit(solution)/shard_map/all_to_all | solution.py:172
  125.7 18.0 %all-gather.3.cloned.1.call-done = bf16[32,48,512]{2,1,0:T(8,128)(2,1)} async-done(((bf16[8,48,512]{2,1,0:T(8,128)(2,1)}), bf16[32,48,512]{2,1,0:T(8,128)(2,1)}) %all-gather.3.cloned.1.call-update) | async-done | bytes 1572880 | tf_op jit(solution)/shard_map/all_gather | solution.py:174
  143.7 2.6 %copy.49 = bf16[8,48,4,512]{3,2,1,0:T(4,128)(2,1)S(1)} copy(bf16[8,48,4,512]{3,1,0,2:T(8,128)(2,1)} %bitcast.81) | data formatting | bytes 3145728 | tf_op jit(solution)/shard_map/reshape | solution.py:174
  146.7 1.1 copy-done.6
  147.9 1.0 fusion.3
  149.5 1.0 fusion.10
  150.5 2.1 %convolution_convert_fusion = bf16[8,48,2048]{2,1,0:T(8,128)(2,1)} fusion(bf16[8,48,512]{2,1,0:T(8,128)(2,1)S(1)} %bitcast.91, bf16[1,512,2048]{2,1,0:T(8,128)(2,1)S(1)} %copy-done), kind=kOutput, calls=%fused_computation.4 | convolution fusion | flops 806092800 | bytes 4063232 | tf_op jit(solution)/shard_map/dot_general | solution.py:180
  152.7 28.1 %reduce-scatter.2.cloned.1.call-done = bf16[8,48,512]{2,1,0:T(8,128)(2,1)} async-done(((bf16[8,48,2048]{2,1,0:T(8,128)(2,1)}), bf16[8,48,512]{2,1,0:T(8,128)(2,1)}) %reduce-scatter.2.cloned.1.call-update) | async-done | bytes 393232 | tf_op jit(solution)/shard_map/reduce_scatter | solution.py:182
  180.8 5.5 %all-to-all-start.1 = ((bf16[8,48,512]{2,1,0:T(8,128)(2,1)}), bf16[8,48,512]{2,1,0:T(8,128)(2,1)S(1)}, u32[]{:S(2)}, u32[]{:S(2)}) async-start(bf16[8,48,512]{2,1,0:T(8,128)(2,1)} %reduce-scatter.2.cloned.1.call-done), calls=%async_computation.2 | async-start | bytes 786432 | tf_op jit(solution)/shard_map/all_to_all | solution.py:185
  186.5 11.4 %all-to-all-done.1 = bf16[8,48,512]{2,1,0:T(8,128)(2,1)S(1)} async-done(((bf16[8,48,512]{2,1,0:T(8,128)(2,1)}), bf16[8,48,512]{2,1,0:T(8,128)(2,1)S(1)}, u32[]{:S(2)}, u32[]{:S(2)}) %all-to-all-start.1) | async-done | bytes 393248 | tf_op jit(solution)/shard_map/all_to_all | solution.py:185
  197.9 1.2 gather_fusion.1
  (73 shorter events, 10.6 us)
Async XLA Ops:
  6.5 144.0 %copy-start = (bf16[1,512,2048]{2,1,0:T(8,128)(2,1)S(1)}, bf16[1,512,2048]{2,1,0:T(8,128)(2,1)}, u32[]{:S(2)}) copy-start(bf16[1,512,2048]{2,1,0:T(8,128)(2,1)} %param.27) | copy-start | bytes 6291460
  6.5 98.8 %all-reduce.2.cloned.1.call-start = ((), (), s32[]{:S(2)}) async-start(), calls=%async_computation.3 | async-start | bytes 1048576 | tf_op jit(solution)/shard_map/psum | solution.py:140
  41.1 1.4 copy-start.1
  43.8 29.1 %copy-start.2 = (bf16[512,2048]{1,0:T(8,128)(2,1)S(1)}, bf16[512,2048]{1,0:T(8,128)(2,1)}, u32[]{:S(2)}) copy-start(bf16[512,2048]{1,0:T(8,128)(2,1)} %param.21) | copy-start | bytes 6291460
  72.9 1.4 copy-start.5
  72.9 32.5 %copy-start.3 = (bf16[128,2048]{1,0:T(8,128)(2,1)S(1)}, bf16[128,2048]{1,0:T(8,128)(2,1)}, u32[]{:S(2)}) copy-start(bf16[128,2048]{1,0:T(8,128)(2,1)} %param.14) | copy-start | bytes 1572868
  74.2 69.4 %all-gather.3.cloned.1.call-start = ((), (), s32[]{:S(2)}) async-start(), calls=%async_computation.5 | async-start | bytes 1966080 | tf_op jit(solution)/shard_map/all_gather | solution.py:174
  125.6 55.2 %reduce-scatter.2.cloned.1.call-start = ((), (), s32[]{:S(2)}) async-start(), calls=%async_computation.4 | async-start | bytes 1966080 | tf_op jit(solution)/shard_map/reduce_scatter | solution.py:182
  146.3 1.6 copy-start.6
  147.9 1.6 copy-start.7
  152.6 33.7 %copy-start.4 = (f32[128,2]{0,1:T(2,128)S(1)}, f32[128,2]{0,1:T(2,128)}, u32[]{:S(2)}) copy-start(f32[128,2]{0,1:T(2,128)} %param.23) | copy-start | bytes 3076
  180.8 17.1 %all-to-all-start.1 = ((bf16[8,48,512]{2,1,0:T(8,128)(2,1)}), bf16[8,48,512]{2,1,0:T(8,128)(2,1)S(1)}, u32[]{:S(2)}, u32[]{:S(2)}) async-start(bf16[8,48,512]{2,1,0:T(8,128)(2,1)} %reduce-scatter.2.cloned.1.call-done), calls=%async_computation.2 | async-start | bytes 786432 | tf_op jit(solution)/shard_map/all_to_all | solution.py:185
Sparse Core Ops, SparseCore 0:
  74.3 30.9 all-reduce.1
  125.8 17.8 all-gather.2
  152.8 27.9 reduce-scatter.1
